TPU v7x, 32 devices: a whole 2x2x4 slice. The times are simulated.
32 devices in a mesh: grp: 2 (over y), fs: 4 (over z), tp: 4 (over x, core).
Axes of the slice: x: 2, y: 2, z: 4, core: 2. Of those that a mesh axis runs over, the one named last changes fastest.
Arguments:
- tokens: bfloat16 [2048, 2048], P(('grp', 'fs'), 'tp'), parts along dimension 0, may hold values from -6 to 6
- route_experts: int32 [2048, 2], P(('grp', 'fs')), parts along dimension 0, may hold values from 0 to 15, as said below
- group_weight: float32 [2048], P(('grp', 'fs')), parts along dimension 0, may hold values from 0.2 to 1
- pair_logit: float32 [2048], P(('grp', 'fs')), parts along dimension 0, may hold values from -6 to 6
- norm_gain: float32 [2048], replicated, may hold values from 0.1 to 1.9
- gate_train: float32 [16, 2048, 2048], P(None, 'fs', 'tp'), may hold values from -0.125 to 0.125
- up_train: float32 [16, 2048, 2048], P(None, 'fs', 'tp'), may hold values from -0.125 to 0.125
- down_train: float32 [16, 2048, 2048], P(None, 'fs', 'tp'), may hold values from -0.125 to 0.125
Outputs:
- gate_serve: bfloat16 [32, 2048, 2048], P(('grp', 'fs'), None, 'tp'), parts along dimension 0
- up_serve: bfloat16 [32, 2048, 2048], P(('grp', 'fs'), None, 'tp'), parts along dimension 0
- down_serve: bfloat16 [32, 2048, 2048], P(('grp', 'fs'), None, 'tp'), parts along dimension 0
- moe_out: bfloat16 [2048, 2048], P(('grp', 'fs'), 'tp'), parts along dimension 0
There are 2 independent parts, one for each index of `grp`. A program takes and returns all parts, laid end to end along the dimension named above; an argument that names none is the same for every part. Nothing has to cross between parts.
Inputs may be any that keep to these rules, and one draw needn't show every extreme that they name: `route_experts`: each row names two different experts of the same group of 4 consecutive expert numbers. Among the 256 aligned rows of one index of fs, no expert is named by more than 64 rows, and in every draw some expert is named by exactly 64 rows from every such block.
All inputs are finite; a program needn't handle non-finite values.
Results may differ from a plain program's by a relative error of at most 0.018.
Values may be sent and summed in bfloat16 or wider, within the bound.
No kernel may reach another device: no remote copies, remote signals or barrier semaphores. Data moves between devices by JAX's collectives and lax.ppermute only.
A program may use at most 192 MiB of HBM per device.

v0:
```python
import jax
import jax.numpy as jnp
from jax import lax
from jax.sharding import PartitionSpec as P

CAP = 64


def shards(
    tokens, route_experts, group_weight, pair_logit, norm_gain, gate_train, up_train, down_train
):
    experts = gate_train.shape[0]
    rows_here = gate_train.shape[1]
    model_width = norm_gain.shape[0]
    owners = lax.axis_size("fs")
    per_owner = experts // owners
    tok_rows = tokens.shape[0]
    slots_all = experts * CAP
    start_row = lax.axis_index("fs") * rows_here
    gain_rows = lax.dynamic_slice_in_dim(norm_gain, start_row, rows_here)
    gate_cast = (gain_rows[None, :, None] * gate_train).astype(jnp.bfloat16)
    up_cast = (gain_rows[None, :, None] * up_train).astype(jnp.bfloat16)
    down_cast = down_train.astype(jnp.bfloat16)
    gate_serve, up_serve, down_serve = (
        lax.all_to_all(gate_cast, "fs", split_axis=0, concat_axis=1, tiled=True),
        lax.all_to_all(up_cast, "fs", split_axis=0, concat_axis=1, tiled=True),
        lax.all_to_all(down_cast, "fs", split_axis=0, concat_axis=1, tiled=True),
    )
    expert_ids = jnp.arange(experts, dtype=jnp.int32)
    flat_hits = (route_experts.reshape(tok_rows * 2)[:, None] == expert_ids[None, :]).astype(
        jnp.int32
    )
    before = jnp.cumsum(flat_hits, axis=0) - flat_hits
    slot_index = jnp.sum(before * flat_hits, axis=1) + CAP * route_experts.reshape(tok_rows * 2)
    placed = (slot_index[:, None] == jnp.arange(slots_all, dtype=jnp.int32)[None, :]).reshape(
        tok_rows, 2, slots_all
    )
    pick_rows = (placed[:, 0] | placed[:, 1]).astype(jnp.bfloat16)
    first_gate = group_weight * jax.nn.sigmoid(pair_logit)
    second_gate = group_weight * jax.nn.sigmoid(-pair_logit)
    combine_weights = (
        placed[:, 0].astype(jnp.float32) * first_gate[:, None]
        + placed[:, 1].astype(jnp.float32) * second_gate[:, None]
    )
    contract_rows = (((0,), (0,)), ((), ()))
    outgoing = lax.dot_general(pick_rows, tokens, contract_rows, preferred_element_type=jnp.float32)
    outgoing = outgoing.astype(jnp.bfloat16).reshape(owners, per_owner, CAP, tokens.shape[1])
    arrived = lax.all_to_all(outgoing, "fs", split_axis=0, concat_axis=0, tiled=True)
    section = lax.all_gather(arrived, "tp", axis=3, tiled=True)
    gate_total = jnp.einsum(
        "sexk,ekf->esxf", section, gate_serve, preferred_element_type=jnp.float32
    )
    up_total = jnp.einsum("sexk,ekf->esxf", section, up_serve, preferred_element_type=jnp.float32)
    squares_total = jnp.sum(jnp.square(section.astype(jnp.float32)), axis=3)
    row_scale = jnp.transpose(lax.rsqrt(squares_total / model_width + 1e-06), (1, 0, 2))[..., None]
    hidden = (jax.nn.silu(row_scale * gate_total) * (row_scale * up_total)).astype(jnp.bfloat16)
    summed = lax.psum_scatter(
        jnp.einsum("edf,esxf->dsex", down_serve, hidden, preferred_element_type=jnp.float32).astype(
            jnp.bfloat16
        ),
        "tp",
        scatter_dimension=0,
        tiled=True,
    )
    returned = lax.all_to_all(summed, "fs", split_axis=1, concat_axis=1, tiled=True)
    flat_back = returned.reshape(returned.shape[0], slots_all).astype(jnp.float32)
    moe_out = lax.dot_general(
        combine_weights,
        flat_back,
        (((1,), (1,)), ((), ())),
        precision=lax.Precision.HIGHEST,
        preferred_element_type=jnp.float32,
    )
    return (gate_serve, up_serve, down_serve, moe_out.astype(jnp.bfloat16))


def solution(mesh):
    in_specs = (
        P(("grp", "fs"), "tp"),
        P(("grp", "fs"), None),
        P(("grp", "fs")),
        P(("grp", "fs")),
        P(),
        P(None, "fs", "tp"),
        P(None, "fs", "tp"),
        P(None, "fs", "tp"),
    )
    out_specs = (
        P(("grp", "fs"), None, "tp"),
        P(("grp", "fs"), None, "tp"),
        P(("grp", "fs"), None, "tp"),
        P(("grp", "fs"), "tp"),
    )
    return jax.shard_map(shards, mesh=mesh, in_specs=in_specs, out_specs=out_specs, check_vma=False)
```

profile of v0, /device:TPU:0, one launch (start us, length us, event | category | flops | bytes accessed | tf_op | source)
XLA Modules:
  0.0 724.7 jit_solution(6965078394565885770)
XLA Ops:
  7.2 0.0 copy-start
  7.2 0.9 copy.42
  8.0 0.1 eq.39
  8.2 0.1 eq.43
  8.3 1.2 reduce-window.6
  9.5 0.2 slice_reduce_fusion
  9.8 0.1 fusion.17
  9.9 0.1 reduce_sum.21
  10.0 0.1 copy.45
  10.1 0.7 multiply_add_fusion
  10.8 0.4 iota_compare_fusion
  11.2 0.0 copy-done
  11.2 1.5 convolution_convert_fusion
  12.7 6.3 all-to-all-start.3
  19.0 0.8 dynamic_slice.3
  19.8 17.1 %multiply_convert_fusion = (bf16[16,512,512]{2,1,0:T(8,128)(2,1)}, bf16[16,512,512]{2,1,0:T(8,128)(2,1)}) fusion(f32[16,512,512]{2,1,0:T(8,128)} %param.14, f32[512]{0:T(512)S(1)} %dynamic_slice.3, f32[16,512,512]{2,1,0:T(8,128)} %param.13), kind=kLoop, calls=%fused_computation | loop fusion | flops 16777216 | bytes 50333696 | tf_op jit(solution)/shard_map/convert_element_type | solution.py:22
  36.9 7.9 %all-to-all-done.3 = bf16[4,4,64,512]{3,2,1,0:T(8,128)(2,1)S(1)} async-done(((bf16[4,4,64,512]{3,2,1,0:T(8,128)(2,1)}), bf16[4,4,64,512]{3,2,1,0:T(8,128)(2,1)S(1)}, u32[]{:S(2)}, u32[]{:S(2)}) %all-to-all-start.3) | async-done | bytes 1048608 | tf_op jit(solution)/shard_map/all_to_all | solution.py:48
  44.8 190.1 %all_to_all.64 = bf16[16,512,512]{2,1,0:T(8,128)(2,1)} all-to-all(bf16[16,512,512]{2,1,0:T(8,128)(2,1)} %get-tuple-element.7), channel_id=1, replica_groups=mesh['grp'=2,'fs'=4,'tp'=4] {'fs'}, dimensions={0} | all-to-all | bytes 16777216 | tf_op jit(solution)/shard_map/all_to_all | solution.py:25
  234.8 5.6 all-to-all-start.1
  240.5 9.0 %convert_element_type.40 = bf16[16,512,512]{2,1,0:T(8,128)(2,1)} convert(f32[16,512,512]{2,1,0:T(8,128)} %param.15) | non-fusion elementwise | flops 4194304 | bytes 25165824 | tf_op jit(solution)/shard_map/convert_element_type | solution.py:23
  249.5 173.1 %all-to-all-done.1 = bf16[16,512,512]{2,1,0:T(8,128)(2,1)} async-done(((bf16[16,512,512]{2,1,0:T(8,128)(2,1)}), bf16[16,512,512]{2,1,0:T(8,128)(2,1)}, u32[]{:S(2)}, u32[]{:S(2)}) %all-to-all-start.1) | async-done | bytes 8388640 | tf_op jit(solution)/shard_map/all_to_all | solution.py:26
  422.6 5.7 all-to-all-start.2
  428.2 0.0 all-gather.2.cloned.1.call-start
  428.3 1.1 copy.46
  429.3 0.0 all-gather.2.cloned.1.call-update
  429.4 0.2 reduce-scatter.2.cloned.1.call-start
  429.6 37.5 %all-gather.2.cloned.1.call-done = bf16[4,4,64,2048]{3,2,0,1:T(8,128)(2,1)} async-done(((bf16[4,4,64,512]{3,2,0,1:T(8,128)(2,1)}), bf16[4,4,64,2048]{3,2,0,1:T(8,128)(2,1)}) %all-gather.2.cloned.1.call-update) | async-done | bytes 4194320 | tf_op jit(solution)/shard_map/all_gather | solution.py:49
  467.1 3.1 multiply_reduce_fusion
  470.2 7.5 %copy.39 = bf16[4,4,512,512]{3,2,0,1:T(8,128)(2,1)} copy(bf16[4,4,512,512]{3,2,1,0:T(8,128)(2,1)} %bitcast.62) | data formatting | bytes 16777216 | tf_op jit(solution)/shard_map/all_to_all | solution.py:25
  477.7 7.5 %copy.40 = bf16[4,4,512,512]{3,2,0,1:T(8,128)(2,1)} copy(bf16[4,4,512,512]{3,2,1,0:T(8,128)(2,1)} %bitcast.3) | data formatting | bytes 16777216 | tf_op jit(solution)/shard_map/all_to_all | solution.py:26
  485.2 125.7 %all-to-all-done.2 = bf16[16,512,512]{2,1,0:T(8,128)(2,1)} async-done(((bf16[16,512,512]{2,1,0:T(8,128)(2,1)}), bf16[16,512,512]{2,1,0:T(8,128)(2,1)}, u32[]{:S(2)}, u32[]{:S(2)}) %all-to-all-start.2) | async-done | bytes 8388640 | tf_op jit(solution)/shard_map/all_to_all | solution.py:27
  610.9 0.0 copy-start.2
  610.9 7.7 %copy.41 = bf16[4,4,512,512]{3,2,0,1:T(8,128)(2,1)} copy(bf16[4,4,512,512]{3,2,1,0:T(8,128)(2,1)} %bitcast.6) | data formatting | bytes 16777216 | tf_op jit(solution)/shard_map/all_to_all | solution.py:27
  618.5 0.0 copy-done.2
  618.5 7.0 fusion.21
  625.6 0.0 copy-start.1
  625.6 14.2 %convert_bitcast_fusion = bf16[2048,4,4,64]{0,3,1,2:T(8,128)(2,1)} fusion(bf16[4,2048,512,1]{2,1,3,0:T(8,128)(2,1)} %bitcast.67, f32[4,4,64,512]{3,2,1,0:T(8,128)} %fusion.21, bf16[4,4,64,2048]{3,2,0,1:T(8,128)(2,1)} %all-gather.2.cloned.1.call-done, bf16[4,2048,512,1]{2,1,3,0:T(8,128)(2,1)} %bitcast.65, f32[4,4,64]{2,1,0:T(4,128)S(1)} %rsqrt_bitcast_fusion), kind=kOutput, calls=%fused_computation.3 | convolution fusion | flops 4301258752 | bytes 27267072 | tf_op jit(solution)/shard_map/edf,esxf->dsex/dot_general | solution.py:58
  639.7 0.0 copy-start.3
  639.7 0.0 copy-start.4
  639.7 0.0 reduce-scatter.2.cloned.1.call-update
  639.8 43.7 %reduce-scatter.2.cloned.1.call-done = bf16[512,4,4,64]{0,3,1,2:T(8,128)(2,1)} async-done(((bf16[2048,4,4,64]{0,3,1,2:T(8,128)(2,1)}), bf16[512,4,4,64]{0,3,1,2:T(8,128)(2,1)}) %reduce-scatter.2.cloned.1.call-update) | async-done | bytes 1048592 | tf_op jit(solution)/shard_map/reduce_scatter | solution.py:57
  683.4 2.3 copy.47
  685.7 4.6 all-to-all-start.4
  690.3 0.0 copy-done.3
  690.3 0.0 copy-done.4
  690.3 25.5 %all-to-all-done.4 = bf16[512,4,4,64]{0,3,2,1:T(8,128)(2,1)S(1)} async-done(((bf16[512,4,4,64]{0,3,2,1:T(8,128)(2,1)}), bf16[512,4,4,64]{0,3,2,1:T(8,128)(2,1)S(1)}, u32[]{:S(2)}, u32[]{:S(2)}) %all-to-all-start.4) | async-done | bytes 1048608 | tf_op jit(solution)/shard_map/all_to_all | solution.py:65
  715.8 2.0 convolution_convert_fusion.1
  717.8 0.0 copy-done.1
  (5 shorter events, 0.1 us)
Async XLA Ops:
  7.2 4.0 copy-start
  12.7 32.1 %all-to-all-start.3 = ((bf16[4,4,64,512]{3,2,1,0:T(8,128)(2,1)}), bf16[4,4,64,512]{3,2,1,0:T(8,128)(2,1)S(1)}, u32[]{:S(2)}, u32[]{:S(2)}) async-start(bf16[4,4,64,512]{3,2,1,0:T(8,128)(2,1)} %bitcast.12), calls=%async_computation.3 | async-start | bytes 2097152 | tf_op jit(solution)/shard_map/all_to_all | solution.py:48
  234.8 187.7 %all-to-all-start.1 = ((bf16[16,512,512]{2,1,0:T(8,128)(2,1)}), bf16[16,512,512]{2,1,0:T(8,128)(2,1)}, u32[]{:S(2)}, u32[]{:S(2)}) async-start(bf16[16,512,512]{2,1,0:T(8,128)(2,1)} %get-tuple-element.6), calls=%async_computation.1 | async-start | bytes 16777216 | tf_op jit(solution)/shard_map/all_to_all | solution.py:26
  422.6 188.3 %all-to-all-start.2 = ((bf16[16,512,512]{2,1,0:T(8,128)(2,1)}), bf16[16,512,512]{2,1,0:T(8,128)(2,1)}, u32[]{:S(2)}, u32[]{:S(2)}) async-start(bf16[16,512,512]{2,1,0:T(8,128)(2,1)} %convert_element_type.40), calls=%async_computation.2 | async-start | bytes 16777216 | tf_op jit(solution)/shard_map/all_to_all | solution.py:27
  428.2 38.8 %all-gather.2.cloned.1.call-start = ((), (), s32[]{:S(2)}) async-start(), calls=%async_computation.6 | async-start | bytes 5242880 | tf_op jit(solution)/shard_map/all_gather | solution.py:49
  429.4 254.0 %reduce-scatter.2.cloned.1.call-start = ((), (), s32[]{:S(2)}) async-start(), calls=%async_computation.7 | async-start | bytes 5242880 | tf_op jit(solution)/shard_map/reduce_scatter | solution.py:57
  610.9 7.7 %copy-start.2 = (bf16[4,4,64,2048]{3,2,0,1:T(8,128)(2,1)S(1)}, bf16[4,4,64,2048]{3,2,0,1:T(8,128)(2,1)}, u32[]{:S(2)}) copy-start(bf16[4,4,64,2048]{3,2,0,1:T(8,128)(2,1)} %all-gather.2.cloned.1.call-done) | copy-start | bytes 12582916
  625.6 92.3 %copy-start.1 = (bf16[256,512]{1,0:T(8,128)(2,1)S(1)}, bf16[256,512]{1,0:T(8,128)(2,1)}, u32[]{:S(2)}) copy-start(bf16[256,512]{1,0:T(8,128)(2,1)} %param.8) | copy-start | bytes 786436
  639.7 50.6 %copy-start.3 = (f32[256]{0:T(256)S(1)}, f32[256]{0:T(256)}, u32[]{:S(2)}) copy-start(f32[256]{0:T(256)} %param.10) | copy-start | bytes 3076
  639.7 50.6 %copy-start.4 = (f32[256]{0:T(256)S(1)}, f32[256]{0:T(256)}, u32[]{:S(2)}) copy-start(f32[256]{0:T(256)} %param.11) | copy-start | bytes 3076
  685.7 30.1 %all-to-all-start.4 = ((bf16[512,4,4,64]{0,3,2,1:T(8,128)(2,1)}), bf16[512,4,4,64]{0,3,2,1:T(8,128)(2,1)S(1)}, u32[]{:S(2)}, u32[]{:S(2)}) async-start(bf16[512,4,4,64]{0,3,2,1:T(8,128)(2,1)} %copy.47), calls=%async_computation.5 | async-start | bytes 2097152 | tf_op jit(solution)/shard_map/all_to_all | solution.py:65
Sparse Core Ops, SparseCore 0:
  431.2 35.8 all-gather.1
  639.9 43.4 reduce-scatter.1
where the time goes:
time: 725 us
  waiting for transfers between devices  413 us (57%)
  blocking collectives  190 us (26%)
  other arithmetic  31.5 us (4%)
  local copies, waits for them, and re-layouts  28.4 us (4%)
  matrix products  24.7 us (3%)
  starting transfers between devices  22.5 us (3%)
  between operations  14.1 us (2%)
    all_to_all x1, blocking collectives, shards(): lax.all_to_all(gate_cast, 'fs', split_axis=0, concat_axis=1, tiled=True)  190 us
    all_to_all x1, waiting for transfers between devices, shards(): lax.all_to_all(up_cast, 'fs', split_axis=0, concat_axis=1, tiled=True)  173 us
    all_to_all x1, waiting for transfers between devices, shards(): lax.all_to_all(down_cast, 'fs', split_axis=0, concat_axis=1, tiled=True)  126 us
    reduce_scatter x1, waiting for transfers between devices, shards(): lax.psum_scatter(jnp.einsum('edf,esxf->dsex', down_serve, hidden, preferr...  43.7 us
    all_gather x1, waiting for transfers between devices, shards(): section = lax.all_gather(arrived, 'tp', axis=3, tiled=True)  37.5 us
    all_to_all x1, waiting for transfers between devices, shards(): lax.all_to_all(summed, 'fs', split_axis=1, concat_axis=1, tiled=True)  25.5 us
    convert_element_type x1, other arithmetic, shards(): up_cast = (gain_rows[None, :, None] * up_train).astype(jnp.bfloat16)  17.1 us
  transfers between devices with their start and end apart: 6, of which 6 were waited for; matrix products, arithmetic and copies ran while one was open for 6% of the time, Pallas kernels for 0%

commit v1 on v0

--- a/solution.py
+++ b/solution.py
@@ -22,7 +22,12 @@
     up_cast = (gain_rows[None, :, None] * up_train).astype(jnp.bfloat16)
     down_cast = down_train.astype(jnp.bfloat16)
     gate_serve, up_serve, down_serve = (
-        lax.all_to_all(gate_cast, "fs", split_axis=0, concat_axis=1, tiled=True),
+        jnp.concatenate(
+            lax.all_to_all(
+                jnp.stack(jnp.split(gate_cast, lax.axis_size("fs"), axis=0)), "fs", 0, 0
+            ),
+            axis=1,
+        ),
         lax.all_to_all(up_cast, "fs", split_axis=0, concat_axis=1, tiled=True),
         lax.all_to_all(down_cast, "fs", split_axis=0, concat_axis=1, tiled=True),
     )

time: 725 us -> 725 us (level)
    all_to_all x1 -> x0, local copies, waits for them, and re-layouts: 7.52 us -> none  [shards(): lax.all_to_all(gate_cast, 'fs', split_axis=0, concat_axis=1, tiled=True)]
    reshape x0 -> x1, local copies, waits for them, and re-layouts: none -> 7.52 us  [shards(): jnp.concatenate(lax.all_to_all(jnp.stack(jnp.split(gate_cast, lax.axis_si...]
  transfers between devices with their start and end apart: 6 -> 6, of which waited for: 6 -> 6; matrix products, arithmetic and copies ran while one was open for 6% -> 7% of each run, Pallas kernels for 0% -> 0%
where the time goes in v1:
time: 725 us
  waiting for transfers between devices  411 us (57%)
  blocking collectives  190 us (26%)
  other arithmetic  33.3 us (5%)
  local copies, waits for them, and re-layouts  29.4 us (4%)
  matrix products  24.7 us (3%)
  starting transfers between devices  22.5 us (3%)
  between operations  14.1 us (2%)
    all_to_all x1, blocking collectives, shards(): lax.all_to_all(jnp.stack(jnp.split(gate_cast, lax.axis_size('fs'), axis=0...  190 us
    all_to_all x1, waiting for transfers between devices, shards(): lax.all_to_all(up_cast, 'fs', split_axis=0, concat_axis=1, tiled=True)  173 us
    all_to_all x1, waiting for transfers between devices, shards(): lax.all_to_all(down_cast, 'fs', split_axis=0, concat_axis=1, tiled=True)  126 us
    reduce_scatter x1, waiting for transfers between devices, shards(): lax.psum_scatter(jnp.einsum('edf,esxf->dsex', down_serve, hidden, preferr...  43.7 us
    all_gather x1, waiting for transfers between devices, shards(): section = lax.all_gather(arrived, 'tp', axis=3, tiled=True)  37.5 us
    all_to_all x1, waiting for transfers between devices, shards(): lax.all_to_all(summed, 'fs', split_axis=1, concat_axis=1, tiled=True)  25.5 us
    convert_element_type x1, other arithmetic, shards(): up_cast = (gain_rows[None, :, None] * up_train).astype(jnp.bfloat16)  15 us
  transfers between devices with their start and end apart: 6, of which 6 were waited for; matrix products, arithmetic and copies ran while one was open for 7% of the time, Pallas kernels for 0%

profile of v1, /device:TPU:0, one launch (start us, length us, event | category | flops | bytes accessed | tf_op | source)
XLA Modules:
  0.0 724.7 jit_solution(15451589766170905185)
XLA Ops:
  7.2 0.0 copy-start
  7.2 0.9 copy.42
  8.0 0.1 eq.39
  8.2 0.1 eq.43
  8.3 1.2 reduce-window.6
  9.5 0.2 slice_reduce_fusion
  9.8 0.1 fusion.17
  9.9 0.1 reduce_sum.21
  10.0 0.1 copy.45
  10.1 0.7 multiply_add_fusion
  10.8 0.4 iota_compare_fusion
  11.2 0.0 copy-done
  11.2 1.5 convolution_convert_fusion
  12.7 6.3 all-to-all-start.3
  19.0 0.8 dynamic_slice.3
  19.8 15.0 %multiply_convert_fusion = (bf16[16,512,512]{2,1,0:T(8,128)(2,1)}, bf16[16,512,512]{2,1,0:T(8,128)(2,1)S(1)}) fusion(f32[16,512,512]{2,1,0:T(8,128)} %param.14, f32[512]{0:T(512)S(1)} %dynamic_slice.3, f32[16,512,512]{2,1,0:T(8,128)} %param.13), kind=kLoop, calls=%fused_computation | loop fusion | flops 16777216 | bytes 50333696 | tf_op jit(solution)/shard_map/convert_element_type | solution.py:22
  34.8 0.9 slice_bitcast_fusion.3
  35.8 3.9 pad_maximum_fusion
  39.6 5.1 all-to-all-done.3
  44.8 190.1 %all_to_all.51 = bf16[4,4,512,512]{3,2,1,0:T(8,128)(2,1)} all-to-all(bf16[4,4,512,512]{3,2,1,0:T(8,128)(2,1)} %pad_maximum_fusion), channel_id=1, replica_groups=mesh['grp'=2,'fs'=4,'tp'=4] {'fs'}, dimensions={0} | all-to-all | bytes 16777216 | tf_op jit(solution)/shard_map/all_to_all | solution.py:26
  234.8 5.6 all-to-all-start.1
  240.5 9.0 %convert_element_type.40 = bf16[16,512,512]{2,1,0:T(8,128)(2,1)} convert(f32[16,512,512]{2,1,0:T(8,128)} %param.15) | non-fusion elementwise | flops 4194304 | bytes 25165824 | tf_op jit(solution)/shard_map/convert_element_type | solution.py:23
  249.4 173.1 %all-to-all-done.1 = bf16[16,512,512]{2,1,0:T(8,128)(2,1)} async-done(((bf16[16,512,512]{2,1,0:T(8,128)(2,1)}), bf16[16,512,512]{2,1,0:T(8,128)(2,1)}, u32[]{:S(2)}, u32[]{:S(2)}) %all-to-all-start.1) | async-done | bytes 8388640 | tf_op jit(solution)/shard_map/all_to_all | solution.py:31
  422.5 5.7 all-to-all-start.2
  428.2 0.0 all-gather.2.cloned.1.call-start
  428.3 1.1 copy.46
  429.3 0.0 all-gather.2.cloned.1.call-update
  429.4 0.2 reduce-scatter.2.cloned.1.call-start
  429.6 37.5 %all-gather.2.cloned.1.call-done = bf16[4,4,64,2048]{3,2,0,1:T(8,128)(2,1)} async-done(((bf16[4,4,64,512]{3,2,0,1:T(8,128)(2,1)}), bf16[4,4,64,2048]{3,2,0,1:T(8,128)(2,1)}) %all-gather.2.cloned.1.call-update) | async-done | bytes 4194320 | tf_op jit(solution)/shard_map/all_gather | solution.py:54
  467.1 3.1 multiply_reduce_fusion
  470.1 7.5 %copy.39 = bf16[4,4,512,512]{3,2,1,0:T(8,128)(2,1)} copy(bf16[4,4,512,512]{3,2,0,1:T(8,128)(2,1)} %bitcast.68) | data formatting | bytes 16777216 | tf_op jit(solution)/shard_map/reshape | solution.py:25
  477.7 7.5 %copy.40 = bf16[4,4,512,512]{3,2,0,1:T(8,128)(2,1)} copy(bf16[4,4,512,512]{3,2,1,0:T(8,128)(2,1)} %bitcast.6) | data formatting | bytes 16777216 | tf_op jit(solution)/shard_map/all_to_all | solution.py:31
  485.2 125.7 %all-to-all-done.2 = bf16[16,512,512]{2,1,0:T(8,128)(2,1)} async-done(((bf16[16,512,512]{2,1,0:T(8,128)(2,1)}), bf16[16,512,512]{2,1,0:T(8,128)(2,1)}, u32[]{:S(2)}, u32[]{:S(2)}) %all-to-all-start.2) | async-done | bytes 8388640 | tf_op jit(solution)/shard_map/all_to_all | solution.py:32
  610.8 0.0 copy-start.2
  610.8 7.7 %copy.41 = bf16[4,4,512,512]{3,2,0,1:T(8,128)(2,1)} copy(bf16[4,4,512,512]{3,2,1,0:T(8,128)(2,1)} %bitcast.9) | data formatting | bytes 16777216 | tf_op jit(solution)/shard_map/all_to_all | solution.py:32
  618.5 0.0 copy-done.2
  618.5 7.0 fusion.21
  625.6 0.0 copy-start.1
  625.6 14.2 %convert_bitcast_fusion = bf16[2048,4,4,64]{0,3,1,2:T(8,128)(2,1)} fusion(bf16[4,2048,512,1]{2,1,3,0:T(8,128)(2,1)} %bitcast.73, f32[4,4,64,512]{3,2,1,0:T(8,128)} %fusion.21, bf16[4,4,64,2048]{3,2,0,1:T(8,128)(2,1)} %all-gather.2.cloned.1.call-done, bf16[4,2048,512,1]{2,1,3,0:T(8,128)(2,1)} %bitcast.71, f32[4,4,64]{2,1,0:T(4,128)S(1)} %rsqrt_bitcast_fusion), kind=kOutput, calls=%fused_computation.4 | convolution fusion | flops 4301258752 | bytes 27267072 | tf_op jit(solution)/shard_map/edf,esxf->dsex/dot_general | solution.py:63
  639.7 0.0 reduce-scatter.2.cloned.1.call-update
  639.7 43.7 %reduce-scatter.2.cloned.1.call-done = bf16[512,4,4,64]{0,3,1,2:T(8,128)(2,1)} async-done(((bf16[2048,4,4,64]{0,3,1,2:T(8,128)(2,1)}), bf16[512,4,4,64]{0,3,1,2:T(8,128)(2,1)}) %reduce-scatter.2.cloned.1.call-update) | async-done | bytes 1048592 | tf_op jit(solution)/shard_map/reduce_scatter | solution.py:62
  683.4 2.3 copy.47
  685.7 4.6 all-to-all-start.4
  690.3 0.0 copy-done.3
  690.3 0.0 copy-done.4
  690.3 25.5 %all-to-all-done.4 = bf16[512,4,4,64]{0,3,2,1:T(8,128)(2,1)S(1)} async-done(((bf16[512,4,4,64]{0,3,2,1:T(8,128)(2,1)}), bf16[512,4,4,64]{0,3,2,1:T(8,128)(2,1)S(1)}, u32[]{:S(2)}, u32[]{:S(2)}) %all-to-all-start.4) | async-done | bytes 1048608 | tf_op jit(solution)/shard_map/all_to_all | solution.py:70
  715.8 2.0 convolution_convert_fusion.1
  717.8 0.0 copy-done.1
  (7 shorter events, 0.1 us)
Async XLA Ops:
  7.2 4.0 copy-start
  12.7 32.1 %all-to-all-start.3 = ((bf16[4,4,64,512]{3,2,1,0:T(8,128)(2,1)}), bf16[4,4,64,512]{3,2,1,0:T(8,128)(2,1)S(1)}, u32[]{:S(2)}, u32[]{:S(2)}) async-start(bf16[4,4,64,512]{3,2,1,0:T(8,128)(2,1)} %bitcast.15), calls=%async_computation.3 | async-start | bytes 2097152 | tf_op jit(solution)/shard_map/all_to_all | solution.py:53
  234.8 187.7 %all-to-all-start.1 = ((bf16[16,512,512]{2,1,0:T(8,128)(2,1)}), bf16[16,512,512]{2,1,0:T(8,128)(2,1)}, u32[]{:S(2)}, u32[]{:S(2)}) async-start(bf16[16,512,512]{2,1,0:T(8,128)(2,1)} %get-tuple-element.10), calls=%async_computation.1 | async-start | bytes 16777216 | tf_op jit(solution)/shard_map/all_to_all | solution.py:31
  422.5 188.3 %all-to-all-start.2 = ((bf16[16,512,512]{2,1,0:T(8,128)(2,1)}), bf16[16,512,512]{2,1,0:T(8,128)(2,1)}, u32[]{:S(2)}, u32[]{:S(2)}) async-start(bf16[16,512,512]{2,1,0:T(8,128)(2,1)} %convert_element_type.40), calls=%async_computation.2 | async-start | bytes 16777216 | tf_op jit(solution)/shard_map/all_to_all | solution.py:32
  428.2 38.8 %all-gather.2.cloned.1.call-start = ((), (), s32[]{:S(2)}) async-start(), calls=%async_computation.6 | async-start | bytes 5242880 | tf_op jit(solution)/shard_map/all_gather | solution.py:54
  429.4 254.1 %reduce-scatter.2.cloned.1.call-start = ((), (), s32[]{:S(2)}) async-start(), calls=%async_computation.7 | async-start | bytes 5242880 | tf_op jit(solution)/shard_map/reduce_scatter | solution.py:62
  610.8 7.7 %copy-start.2 = (bf16[4,4,64,2048]{3,2,0,1:T(8,128)(2,1)S(1)}, bf16[4,4,64,2048]{3,2,0,1:T(8,128)(2,1)}, u32[]{:S(2)}) copy-start(bf16[4,4,64,2048]{3,2,0,1:T(8,128)(2,1)} %all-gather.2.cloned.1.call-done) | copy-start | bytes 12582916
  625.6 92.3 %copy-start.1 = (bf16[256,512]{1,0:T(8,128)(2,1)S(1)}, bf16[256,512]{1,0:T(8,128)(2,1)}, u32[]{:S(2)}) copy-start(bf16[256,512]{1,0:T(8,128)(2,1)} %param.8) | copy-start | bytes 786436
  639.7 50.6 %copy-start.3 = (f32[256]{0:T(256)S(1)}, f32[256]{0:T(256)}, u32[]{:S(2)}) copy-start(f32[256]{0:T(256)} %param.10) | copy-start | bytes 3076
  639.7 50.6 %copy-start.4 = (f32[256]{0:T(256)S(1)}, f32[256]{0:T(256)}, u32[]{:S(2)}) copy-start(f32[256]{0:T(256)} %param.11) | copy-start | bytes 3076
  685.7 30.1 %all-to-all-start.4 = ((bf16[512,4,4,64]{0,3,2,1:T(8,128)(2,1)}), bf16[512,4,4,64]{0,3,2,1:T(8,128)(2,1)S(1)}, u32[]{:S(2)}, u32[]{:S(2)}) async-start(bf16[512,4,4,64]{0,3,2,1:T(8,128)(2,1)} %copy.47), calls=%async_computation.5 | async-start | bytes 2097152 | tf_op jit(solution)/shard_map/all_to_all | solution.py:70
Sparse Core Ops, SparseCore 0:
  431.2 35.8 all-gather.1
  639.9 43.4 reduce-scatter.1
